TPU v7x, 32 devices: a whole 2x2x4 slice. The times are simulated.
32 devices in a mesh: grp: 2 (over y), sp: 4 (over z), tp: 4 (over x, core).
Axes of the slice: x: 2, y: 2, z: 4, core: 2. Of those that a mesh axis runs over, the one named last changes fastest.
Arguments:
- tokens: bfloat16 [256, 8, 2048], P(('sp', 'tp'), 'grp'), parts along dimension 1, may hold values from -6 to 6
- norm_gain: float32 [2048], replicated, may hold values from 0.1 to 1.9
- w_query: bfloat16 [2048, 2048], P('sp', 'tp'), may hold values from -0.125 to 0.125
- w_value: bfloat16 [2048, 2048], P('sp', 'tp'), may hold values from -0.125 to 0.125
- w_fwd_gate: bfloat16 [2048, 2048], P('sp', 'tp'), may hold values from -0.125 to 0.125
- w_bwd_gate: bfloat16 [2048, 2048], P('sp', 'tp'), may hold values from -0.125 to 0.125
- w_out_gate: bfloat16 [2048, 2048], P('sp', 'tp'), may hold values from -0.125 to 0.125
- floor_gap: float32 [2, 2048], P(None, 'tp'), may hold values from 0.00078125 to 0.1
- decay_shift: float32 [256, 8, 2048], P('sp', 'grp', 'tp'), parts along dimension 1, may hold values from -1.1 to 0
- head_gain: float32 [128], replicated, may hold values from 0.1 to 1.9
- w_out: bfloat16 [2048, 2048], P('tp', 'sp'), may hold values from -0.125 to 0.125
Outputs:
- layer_out: bfloat16 [256, 8, 2048], P(('sp', 'tp'), 'grp'), parts along dimension 1
There are 2 independent parts, one for each index of `grp`. A program takes and returns all parts, laid end to end along the dimension named above; an argument that names none is the same for every part. Nothing has to cross between parts.
All inputs are finite; a program needn't handle non-finite values.
Results may differ from a plain program's by a relative error of at most 0.013.
Values may be sent and summed in bfloat16 or wider, within the bound.
A program may use at most 128 MiB of HBM per device.

v0:
```python
import jax
import jax.numpy as jnp
from jax import lax
from jax.sharding import PartitionSpec as P

KEY = 128
VAL = 128
BLOCK = 64
norm_eps = 1e-06
highest = lax.Precision.HIGHEST


def carried_in(x, axis, join, neutral, backward):
    count = lax.axis_size(axis)
    place = lax.axis_index(axis)
    ahead = count - 1 - place if backward else place
    gathered = jax.tree.map(
        lambda a, kind: lax.all_gather(a.astype(kind), axis), x, (jnp.bfloat16, jnp.bfloat16)
    )
    state = jax.tree.map(lambda a, e: jnp.zeros_like(a) + jnp.asarray(e, a.dtype), x, neutral)

    def one(turn, state):
        source = count - 1 - turn if backward else turn
        return join(
            state,
            jax.tree.map(
                lambda a, own: lax.dynamic_index_in_dim(a, source, 0, False).astype(own.dtype),
                gathered,
                x,
            ),
        )

    return lax.fori_loop(0, ahead, one, state)


def split_blocks(array):
    return array.reshape(array.shape[0] // BLOCK, BLOCK, *array.shape[1:])


def prepare_chain(queries, key_cols, values, log_decay):
    query_blocks = split_blocks(queries)
    key_blocks = split_blocks(key_cols)
    value_blocks = split_blocks(values)
    running = jnp.cumsum(split_blocks(log_decay), axis=1)
    block_end = running[:, -1]
    block_state = jnp.einsum(
        "nsbhk,nsbhe->nbhke",
        key_blocks * jnp.exp(block_end[:, None] - running),
        value_blocks,
        precision=highest,
    )
    carry_state = jnp.zeros_like(block_state[0])
    log_total = jnp.zeros_like(block_end[0])
    offsets = [log_total]
    carry_state = jnp.exp(block_end[0])[..., None] * carry_state + block_state[0]
    log_total = block_end[0]
    return (
        query_blocks,
        key_blocks,
        value_blocks,
        running,
        block_state,
        jnp.stack(offsets),
        log_total,
        carry_state,
    )


def local_pass(chain, carry_state):
    query_blocks, key_blocks, value_blocks, running, block_state = (
        chain[0],
        chain[1],
        chain[2],
        chain[3],
        chain[4],
    )
    block_len = running.shape[1]
    earlier_mask = jnp.arange(block_len)[:, None] >= jnp.arange(block_len)[None, :]
    here = running[0]
    anchor = here[:1]
    query_scaled = query_blocks[0] * jnp.exp(here - anchor)
    key_scaled = key_blocks[0] * jnp.exp(anchor - here)
    scores = jnp.einsum("tbhk,sbhk->bhts", query_scaled, key_scaled, precision=highest)
    scores = jnp.where(earlier_mask, scores, 0.0)
    within = jnp.einsum("bhts,sbhe->tbhe", scores, value_blocks[0], precision=highest)
    carried = jnp.einsum(
        "tbhk,bhke->tbhe", query_blocks[0] * jnp.exp(here), carry_state, precision=highest
    )
    outputs = within + carried
    return outputs


def combine(earlier, later):
    return (earlier[0] + later[0], jnp.exp(later[0])[..., None] * earlier[1] + later[1])


def group_sums(flat_mixed, weight_lines, group_count):
    group_width = flat_mixed.shape[1] // group_count
    accumulated_total = jnp.zeros((flat_mixed.shape[0], weight_lines.shape[1]), jnp.float32)
    for tp_group in range(group_count):
        first_column = tp_group * group_width
        partial_value = jnp.dot(
            flat_mixed[:, first_column : first_column + group_width],
            weight_lines[first_column : first_column + group_width],
            preferred_element_type=jnp.float32,
        ).astype(jnp.bfloat16)
        accumulated_total = accumulated_total + lax.optimization_barrier(partial_value).astype(
            jnp.float32
        )
    return accumulated_total


def shards(
    tokens,
    norm_gain,
    w_query,
    w_value,
    w_fwd_gate,
    w_bwd_gate,
    w_out_gate,
    floor_gap,
    decay_shift,
    head_gain,
    w_out,
):
    token_f32 = tokens.astype(jnp.float32)
    scale_rows = lax.rsqrt(jnp.mean(token_f32 * token_f32, axis=-1, keepdims=True) + norm_eps)
    normed = (token_f32 * scale_rows * norm_gain).astype(jnp.bfloat16)
    weights = (
        lax.all_gather(w_query, "sp", axis=0, tiled=True),
        lax.all_gather(w_value, "sp", axis=0, tiled=True),
        lax.all_gather(w_fwd_gate, "sp", axis=0, tiled=True),
        lax.all_gather(w_bwd_gate, "sp", axis=0, tiled=True),
        lax.all_gather(w_out_gate, "sp", axis=0, tiled=True),
    )
    piece_rows = lax.all_gather(normed, "tp", axis=0, tiled=True)
    flat_rows = piece_rows.reshape(-1, piece_rows.shape[2])
    columns = [
        jnp.dot(flat_rows, matrix, preferred_element_type=jnp.float32).astype(jnp.bfloat16)
        for matrix in weights
    ]
    projected = lax.optimization_barrier(
        jnp.concatenate(columns, axis=1).reshape(piece_rows.shape[0], piece_rows.shape[1], -1)
    )
    key_width = w_query.shape[1]
    value_width = w_value.shape[1]
    heads_here = key_width // KEY
    extent_rows = projected.shape[0]
    seq_count = projected.shape[1]
    bounds_list = [
        0,
        key_width,
        key_width + value_width,
        2 * key_width + value_width,
        3 * key_width + value_width,
        3 * key_width + 2 * value_width,
    ]

    def section_part(position, feature_lanes):
        picked = projected[:, :, bounds_list[position] : bounds_list[position + 1]].astype(
            jnp.float32
        )
        return picked.reshape(extent_rows, seq_count, heads_here, feature_lanes)

    queries = jax.nn.silu(section_part(0, KEY))
    values = section_part(1, VAL)
    shift = decay_shift.reshape(extent_rows, seq_count, heads_here, KEY)
    key_fwd = floor_gap[0].reshape(heads_here, KEY) * jax.nn.sigmoid(-section_part(2, KEY))
    key_bwd = floor_gap[1].reshape(heads_here, KEY) * jax.nn.sigmoid(-section_part(3, KEY))
    decay_fwd = jnp.log1p(-key_fwd) + shift
    decay_bwd = jnp.log1p(-key_bwd) + shift
    fwd_chain = prepare_chain(queries, key_fwd, values, decay_fwd)
    bwd_chain = prepare_chain(queries[::-1], key_bwd[::-1], values[::-1], decay_bwd[::-1])
    identity_pair = (jnp.zeros_like(fwd_chain[6]), jnp.zeros_like(fwd_chain[7]))
    fwd_in = carried_in((fwd_chain[6], fwd_chain[7]), "sp", combine, identity_pair, False)[1]
    bwd_in = carried_in((bwd_chain[6], bwd_chain[7]), "sp", combine, identity_pair, True)[1]
    out_fwd = local_pass(fwd_chain, fwd_in)
    out_bwd = local_pass(bwd_chain, bwd_in)
    combined = out_fwd + out_bwd[::-1]
    head_normed = (
        combined
        * lax.rsqrt(jnp.mean(combined * combined, axis=-1, keepdims=True) + norm_eps)
        * head_gain
    )
    gate_value = jax.nn.silu(projected[:, :, bounds_list[4] : bounds_list[5]].astype(jnp.float32))
    mixed = (head_normed.reshape(extent_rows, seq_count, value_width) * gate_value).astype(
        jnp.bfloat16
    )
    token_rows = lax.all_to_all(mixed, "tp", split_axis=0, concat_axis=2, tiled=True)
    flat_mixed = token_rows.reshape(-1, token_rows.shape[2])
    group_count = lax.axis_size("tp")
    w_columns = lax.all_gather(w_out, "sp", axis=1, tiled=True)
    w_full = lax.all_gather(w_columns, "tp", axis=0, tiled=True)
    accumulated_total = group_sums(flat_mixed, w_full, group_count)
    result = accumulated_total.reshape(token_rows.shape[0], token_rows.shape[1], -1)
    return result.astype(jnp.bfloat16)


def solution(mesh):
    return jax.shard_map(
        shards,
        mesh=mesh,
        in_specs=(
            P(("sp", "tp"), "grp", None),
            P(),
            P("sp", "tp"),
            P("sp", "tp"),
            P("sp", "tp"),
            P("sp", "tp"),
            P("sp", "tp"),
            P(None, "tp"),
            P("sp", "grp", "tp"),
            P(),
            P("tp", "sp"),
        ),
        out_specs=P(("sp", "tp"), "grp", None),
        check_vma=False,
    )
```

profile of v0, /device:TPU:25, one launch (start us, length us, event | category | flops | bytes accessed | tf_op | source)
XLA Modules:
  0.0 473.5 jit_solution(7733809750445567502)
XLA Ops:
  6.5 1.2 fusion.14
  7.8 1.9 fusion.16
  9.7 0.7 all-gather.17.cloned.1.call-update
  13.7 1.1 reshape.201
  15.1 12.7 %all-gather.15.cloned.1.call-done = bf16[64,4,2048]{2,1,0:T(4,128)(2,1)} async-done(((bf16[16,4,2048]{2,1,0:T(4,128)(2,1)}), bf16[64,4,2048]{2,1,0:T(4,128)(2,1)}) %all-gather.15.cloned.1.call-update) | async-done | bytes 1048592 | tf_op jit(solution)/shard_map/all_gather | solution.py:136
  27.9 1.3 reshape.197
  29.2 43.8 %all-gather.17.cloned.1.call-done = bf16[2048,512]{1,0:T(8,128)(2,1)} async-done(((bf16[512,512]{1,0:T(8,128)(2,1)}), bf16[2048,512]{1,0:T(8,128)(2,1)}) %all-gather.17.cloned.1.call-update) | async-done | bytes 2097168 | tf_op jit(solution)/shard_map/all_gather | solution.py:130
  73.0 3.0 fusion.9
  76.0 43.0 %all-gather.19.cloned.1.call-done = bf16[2048,512]{1,0:T(8,128)(2,1)} async-done(((bf16[512,512]{1,0:T(8,128)(2,1)}), bf16[2048,512]{1,0:T(8,128)(2,1)}) %all-gather.19.cloned.1.call-update) | async-done | bytes 2097168 | tf_op jit(solution)/shard_map/all_gather | solution.py:131
  119.0 3.0 fusion.10
  122.1 42.9 %all-gather.21.cloned.1.call-done = bf16[2048,512]{1,0:T(8,128)(2,1)} async-done(((bf16[512,512]{1,0:T(8,128)(2,1)}), bf16[2048,512]{1,0:T(8,128)(2,1)}) %all-gather.21.cloned.1.call-update) | async-done | bytes 2097168 | tf_op jit(solution)/shard_map/all_gather | solution.py:132
  165.0 3.0 fusion.11
  168.0 42.9 %all-gather.23.cloned.1.call-done = bf16[2048,512]{1,0:T(8,128)(2,1)} async-done(((bf16[512,512]{1,0:T(8,128)(2,1)}), bf16[2048,512]{1,0:T(8,128)(2,1)}) %all-gather.23.cloned.1.call-update) | async-done | bytes 2097168 | tf_op jit(solution)/shard_map/all_gather | solution.py:133
  210.9 3.0 fusion.12
  213.9 42.9 %all-gather.25.cloned.1.call-done = bf16[2048,512]{1,0:T(8,128)(2,1)} async-done(((bf16[512,512]{1,0:T(8,128)(2,1)}), bf16[2048,512]{1,0:T(8,128)(2,1)}) %all-gather.25.cloned.1.call-update) | async-done | bytes 2097168 | tf_op jit(solution)/shard_map/all_gather | solution.py:134
  256.8 3.0 fusion.13
  259.8 2.6 reshape.198
  262.4 1.1 fusion.62
  263.7 1.0 div.48
  264.7 1.1 reshape.209
  266.2 1.2 log-plus-one_add_fusion
  267.8 3.0 fusion.36
  270.8 1.5 fusion.26
  272.4 2.8 fusion.5
  275.5 1.0 reshape.214
  276.5 2.5 fusion.35
  278.9 2.0 fusion.4
  281.0 21.8 %all-gather.27.cloned.1.call-done = bf16[512,2048]{1,0:T(8,128)(2,1)} async-done(((bf16[512,512]{1,0:T(8,128)(2,1)}), bf16[512,2048]{1,0:T(8,128)(2,1)}) %all-gather.27.cloned.1.call-update) | async-done | bytes 2097168 | tf_op jit(solution)/shard_map/all_gather | solution.py:192
  302.9 10.5 %all-gather = bf16[4,1,4,4,128]{4,3,2,1,0:T(4,128)(2,1)S(1)} all-gather(bf16[1,1,4,4,128]{4,3,2,1,0:T(4,128)(2,1)S(1)} %slice.123), channel_id=2, replica_groups=mesh['grp'=2,'sp'=4,'tp'=4] {'sp'}, dimensions={0}, use_global_device_ids=true | all-gather | bytes 20480 | tf_op jit(solution)/shard_map/all_gather | solution.py:18
  313.4 10.9 %all-gather.2 = bf16[4,1,4,4,128]{4,3,2,1,0:T(4,128)(2,1)S(1)} all-gather(bf16[1,1,4,4,128]{4,3,2,1,0:T(4,128)(2,1)S(1)} %slice.122), channel_id=4, replica_groups=mesh['grp'=2,'sp'=4,'tp'=4] {'sp'}, dimensions={0}, use_global_device_ids=true | all-gather | bytes 20480 | tf_op jit(solution)/shard_map/all_gather | solution.py:18
  324.2 2.4 convolution_select_fusion.1
  326.7 1.2 fusion.56
  327.9 1.2 convolution_select_fusion
  329.7 19.4 %all-gather.33.cloned.1.call-done = bf16[16,4,128,128]{3,2,1,0:T(8,128)(2,1)} async-done(((bf16[4,4,128,128]{3,2,1,0:T(8,128)(2,1)}), bf16[16,4,128,128]{3,2,1,0:T(8,128)(2,1)}) %all-gather.33.cloned.1.call-update) | async-done | bytes 2097168 | tf_op jit(solution)/shard_map/all_gather | solution.py:18
  349.2 1.1 fusion.6
  350.4 44.8 %all-gather.31.cloned.1.call-done = bf16[16,4,128,128]{3,2,1,0:T(8,128)(2,1)} async-done(((bf16[4,4,128,128]{3,2,1,0:T(8,128)(2,1)}), bf16[16,4,128,128]{3,2,1,0:T(8,128)(2,1)}) %all-gather.31.cloned.1.call-update) | async-done | bytes 2097168 | tf_op jit(solution)/shard_map/all_gather | solution.py:18
  395.4 4.9 %while.26 = (s32[]{:T(128)}, f32[4,4,128,128]{3,2,1,0:T(8,128)S(1)}, s32[]{:T(128)}, bf16[4,4,4,128]{3,2,1,0:T(4,128)(2,1)S(1)}, bf16[4,4,4,128,128]{4,3,2,1,0:T(8,128)(2,1)}, /*index=5*/s32[]{:T(128)}, s32[]{:T(128)}, s32[]{:T(128)}) while((s32[]{:T(128)}, f32[4,4,128,128]{3,2,1,0:T(8,128)S(1)}, s32[]{:T(128)}, ...), condition=%wide.region_3.4_spmd, body=%wide.region_2.3_spmd.sunk | while | flops 788485 | bytes 2642047 | solution.py:33
  395.4 1.6 convert_add_fusion.4
  397.1 1.5 convert_add_fusion.4
  398.7 1.5 convert_add_fusion.4
  400.3 1.2 multiply_reduce_fusion
  402.0 9.5 %all_to_all.15 = bf16[64,4,512]{2,1,0:T(4,128)(2,1)S(1)} all-to-all(bf16[64,4,512]{2,1,0:T(4,128)(2,1)S(1)} %copy.53), channel_id=1, replica_groups=mesh['grp'=2,'sp'=4,'tp'=4] {'tp'}, dimensions={0} | all-to-all | bytes 524288 | tf_op jit(solution)/shard_map/all_to_all | solution.py:189
  411.8 45.6 %all-gather.29.cloned.1.call-done = bf16[2048,2048]{1,0:T(8,128)(2,1)} async-done(((bf16[512,2048]{1,0:T(8,128)(2,1)}), bf16[2048,2048]{1,0:T(8,128)(2,1)}) %all-gather.29.cloned.1.call-update) | async-done | bytes 8388624 | tf_op jit(solution)/shard_map/all_gather | solution.py:193
  457.4 2.1 convolution_convert_fusion.3
  459.5 2.1 convolution_convert_fusion.2
  461.5 2.1 convolution_convert_fusion.1
  463.6 2.1 convolution_convert_fusion
  465.8 0.8 convert_element_type.171
  (69 shorter events, 6.6 us)
Async XLA Ops:
  6.5 7.2 %copy-start.3 = (f32[64,4,512]{2,1,0:T(4,128)S(1)}, f32[64,4,512]{2,1,0:T(4,128)}, u32[]{:S(2)}) copy-start(f32[64,4,512]{2,1,0:T(4,128)} %param.23) | copy-start | bytes 1572868
  6.5 21.3 %all-gather.15.cloned.1.call-start = ((), (), s32[]{:S(2)}) async-start(), calls=%async_computation.1 | async-start | bytes 1310720 | tf_op jit(solution)/shard_map/all_gather | solution.py:136
  9.7 63.3 %all-gather.17.cloned.1.call-start = ((), (), s32[]{:S(2)}) async-start(), calls=%async_computation.2 | async-start | bytes 2621440 | tf_op jit(solution)/shard_map/all_gather | solution.py:130
  10.4 108.6 %all-gather.19.cloned.1.call-start = ((), (), s32[]{:S(2)}) async-start(), calls=%async_computation.3 | async-start | bytes 2621440 | tf_op jit(solution)/shard_map/all_gather | solution.py:131
  11.1 4.0 copy-start.7
  11.2 153.8 %all-gather.21.cloned.1.call-start = ((), (), s32[]{:S(2)}) async-start(), calls=%async_computation.4 | async-start | bytes 2621440 | tf_op jit(solution)/shard_map/all_gather | solution.py:132
  11.7 199.1 %all-gather.23.cloned.1.call-start = ((), (), s32[]{:S(2)}) async-start(), calls=%async_computation.5 | async-start | bytes 2621440 | tf_op jit(solution)/shard_map/all_gather | solution.py:133
  12.3 244.5 %all-gather.25.cloned.1.call-start = ((), (), s32[]{:S(2)}) async-start(), calls=%async_computation.6 | async-start | bytes 2621440 | tf_op jit(solution)/shard_map/all_gather | solution.py:134
  12.9 290.0 %all-gather.27.cloned.1.call-start = ((), (), s32[]{:S(2)}) async-start(), calls=%async_computation.7 | async-start | bytes 2621440 | tf_op jit(solution)/shard_map/all_gather | solution.py:192
  13.6 335.5 %all-gather.33.cloned.1.call-start = ((), (), s32[]{:S(2)}) async-start(), calls=%async_computation.10 | async-start | bytes 2621440 | tf_op jit(solution)/shard_map/all_gather | solution.py:18
  267.7 3.2 copy-start.2
  275.2 120.0 %all-gather.31.cloned.1.call-start = ((), (), s32[]{:S(2)}) async-start(), calls=%async_computation.9 | async-start | bytes 2621440 | tf_op jit(solution)/shard_map/all_gather | solution.py:18
  281.0 176.4 %all-gather.29.cloned.1.call-start = ((), (), s32[]{:S(2)}) async-start(), calls=%async_computation.8 | async-start | bytes 10485760 | tf_op jit(solution)/shard_map/all_gather | solution.py:193
  302.9 25.0 %copy-start = (f32[64,4,4,128]{3,2,1,0:T(4,128)S(1)}, f32[64,4,4,128]{3,2,1,0:T(4,128)}, u32[]{:S(2)}) copy-start(f32[64,4,4,128]{3,2,1,0:T(4,128)} %get-tuple-element.169) | copy-start | bytes 1572868
  302.9 25.0 %copy-start.1 = (f32[64,4,4,128]{3,2,1,0:T(4,128)S(1)}, f32[64,4,4,128]{3,2,1,0:T(4,128)}, u32[]{:S(2)}) copy-start(f32[64,4,4,128]{3,2,1,0:T(4,128)} %get-tuple-element.170) | copy-start | bytes 1572868
  395.4 4.9 %copy-start.4 = (f32[4,4,128,64]{2,3,1,0:T(8,128)S(1)}, f32[4,4,128,64]{2,3,1,0:T(8,128)}, u32[]{:S(2)}) copy-start(f32[4,4,128,64]{2,3,1,0:T(8,128)} %fusion.56) | copy-start | bytes 1572868
  395.4 4.9 %copy-start.5 = (f32[64,4,4,128]{3,2,1,0:T(4,128)S(1)}, f32[64,4,4,128]{3,2,1,0:T(4,128)}, u32[]{:S(2)}) copy-start(f32[64,4,4,128]{3,2,1,0:T(4,128)} %get-tuple-element.155) | copy-start | bytes 1572868
  400.3 1.3 copy-start.6
  400.3 1.3 copy-start.8
Sparse Core Ops, SparseCore 0:
  9.8 18.0 all-gather.14
  29.4 43.4 all-gather.16
  74.5 44.4 all-gather.18
  120.5 44.4 all-gather.20
  166.4 44.4 all-gather.22
  212.3 44.4 all-gather.24
  258.4 44.4 all-gather.26
  304.4 44.6 all-gather.32
  350.7 44.5 all-gather.30
  396.7 60.6 all-gather.28
where the time goes:
time: 474 us; the launch traced here: 473 us
  waiting for transfers between devices  364 us (77%)
  matrix products  36.1 us (8%)
  blocking collectives  30.8 us (6%)
  other arithmetic  18.1 us (4%)
  between operations  13.9 us (3%)
  local copies, waits for them, and re-layouts  10.4 us (2%)
    all_gather x2, waiting for transfers between devices, carried_in(): lax.all_gather(a.astype(kind), axis)  64.2 us
    all_gather x1, waiting for transfers between devices, shards(): w_full = lax.all_gather(w_columns, 'tp', axis=0, tiled=True)  45.6 us
    all_gather x1, waiting for transfers between devices, shards(): lax.all_gather(w_query, 'sp', axis=0, tiled=True)  43.8 us
    all_gather x1, waiting for transfers between devices, shards(): lax.all_gather(w_value, 'sp', axis=0, tiled=True)  43 us
    all_gather x1, waiting for transfers between devices, shards(): lax.all_gather(w_out_gate, 'sp', axis=0, tiled=True)  42.9 us
    all_gather x1, waiting for transfers between devices, shards(): lax.all_gather(w_bwd_gate, 'sp', axis=0, tiled=True)  42.9 us
    all_gather x1, waiting for transfers between devices, shards(): lax.all_gather(w_fwd_gate, 'sp', axis=0, tiled=True)  42.9 us
    all_gather x1, waiting for transfers between devices, shards(): w_columns = lax.all_gather(w_out, 'sp', axis=1, tiled=True)  21.8 us
  transfers between devices with their start and end apart: 10, of which 10 were waited for; matrix products, arithmetic and copies ran while one was open for 11% of the time, Pallas kernels for 0%

commit v1 on v0

--- a/solution.py
+++ b/solution.py
@@ -190,7 +190,12 @@
     flat_mixed = token_rows.reshape(-1, token_rows.shape[2])
     group_count = lax.axis_size("tp")
     w_columns = lax.all_gather(w_out, "sp", axis=1, tiled=True)
-    w_full = lax.all_gather(w_columns, "tp", axis=0, tiled=True)
+    ring = [w_columns]
+    for hop in range(3):
+        ring.append(lax.ppermute(ring[-1], "tp", [(dev, (dev + 1) % 4) for dev in range(4)]))
+    w_full = jnp.roll(
+        jnp.concatenate(ring[::-1], axis=0), (lax.axis_index("tp") + 1) * ring[0].shape[0], axis=0
+    )
     accumulated_total = group_sums(flat_mixed, w_full, group_count)
     result = accumulated_total.reshape(token_rows.shape[0], token_rows.shape[1], -1)
     return result.astype(jnp.bfloat16)

time: 474 us -> 433 us (0.914)
  waiting for transfers between devices: 364 us -> 311 us
  starting transfers between devices: 0.54 us -> 13.8 us
  local copies, waits for them, and re-layouts: 10.4 us -> 22.7 us
  blocking collectives: 30.8 us -> 21.7 us
  matrix products: 36.1 us -> 30.1 us
    all_gather x1 -> x0, waiting for transfers between devices: 45.6 us -> none  [shards(): w_full = lax.all_gather(w_columns, 'tp', axis=0, tiled=True)]
    all_gather x2, waiting for transfers between devices: 64.2 us -> 27.3 us  [carried_in(): lax.all_gather(a.astype(kind), axis)]
    ppermute x0 -> x3, waiting for transfers between devices: none -> 14 us  [shards(): lax.ppermute(ring[-1], 'tp', [(dev, (dev + 1) % 4) for dev in range(4)])]
    unnamed x19 -> x34, local copies, waits for them, and re-layouts: 0.09 us -> 9.77 us
    ppermute x0 -> x3, starting transfers between devices: none -> 9.57 us  [shards(): lax.ppermute(ring[-1], 'tp', [(dev, (dev + 1) % 4) for dev in range(4)])]
    all_to_all x1 -> x0, blocking collectives: 9.49 us -> none  [shards(): lax.all_to_all(mixed, 'tp', split_axis=0, concat_axis=2, tiled=True)]
    all_gather x1, waiting for transfers between devices: 21.8 us -> 30.3 us  [shards(): w_columns = lax.all_gather(w_out, 'sp', axis=1, tiled=True)]
    dot_general x4, matrix products: 8.28 us -> 1.95 us  [group_sums(): jnp.dot(flat_mixed[:, first_column:first_column + group_width], weight_li...]
  transfers between devices with their start and end apart: 10 -> 13, of which waited for: 10 -> 11; matrix products, arithmetic and copies ran while one was open for 11% -> 13% of each run, Pallas kernels for 0% -> 0%
where the time goes in v1:
time: 433 us; the launch traced here: 432 us
  waiting for transfers between devices  311 us (72%)
  matrix products  30.1 us (7%)
  local copies, waits for them, and re-layouts  22.7 us (5%)
  blocking collectives  21.7 us (5%)
  other arithmetic  18.5 us (4%)
  starting transfers between devices  13.8 us (3%)
  between operations  13.7 us (3%)
    all_gather x1, waiting for transfers between devices, shards(): lax.all_gather(w_value, 'sp', axis=0, tiled=True)  43.8 us
    all_gather x1, waiting for transfers between devices, shards(): lax.all_gather(w_query, 'sp', axis=0, tiled=True)  43.8 us
    all_gather x1, waiting for transfers between devices, shards(): lax.all_gather(w_fwd_gate, 'sp', axis=0, tiled=True)  43.6 us
    all_gather x1, waiting for transfers between devices, shards(): lax.all_gather(w_out_gate, 'sp', axis=0, tiled=True)  43.6 us
    all_gather x1, waiting for transfers between devices, shards(): lax.all_gather(w_bwd_gate, 'sp', axis=0, tiled=True)  43.6 us
    all_gather x1, waiting for transfers between devices, shards(): w_columns = lax.all_gather(w_out, 'sp', axis=1, tiled=True)  30.3 us
    all_gather x2, waiting for transfers between devices, carried_in(): lax.all_gather(a.astype(kind), axis)  27.3 us
    all_gather x2, blocking collectives, carried_in(): lax.all_gather(a.astype(kind), axis)  21.7 us
  transfers between devices with their start and end apart: 13, of which 11 were waited for; matrix products, arithmetic and copies ran while one was open for 13% of the time, Pallas kernels for 0%

profile of v1, /device:TPU:25, one launch (start us, length us, event | category | flops | bytes accessed | tf_op | source)
XLA Modules:
  0.0 432.0 jit_solution(5856848597347600547)
XLA Ops:
  6.5 1.2 fusion.14
  7.8 1.9 fusion.16
  15.1 12.8 %all-gather.14.cloned.1.call-done = bf16[64,4,2048]{2,1,0:T(4,128)(2,1)} async-done(((bf16[16,4,2048]{2,1,0:T(4,128)(2,1)}), bf16[64,4,2048]{2,1,0:T(4,128)(2,1)}) %all-gather.14.cloned.1.call-update) | async-done | bytes 1048592 | tf_op jit(solution)/shard_map/all_gather | solution.py:136
  27.9 1.3 reshape.197
  29.2 43.8 %all-gather.16.cloned.1.call-done = bf16[2048,512]{1,0:T(8,128)(2,1)} async-done(((bf16[512,512]{1,0:T(8,128)(2,1)}), bf16[2048,512]{1,0:T(8,128)(2,1)}) %all-gather.16.cloned.1.call-update) | async-done | bytes 2097168 | tf_op jit(solution)/shard_map/all_gather | solution.py:130
  73.0 2.3 fusion.9
  75.3 43.8 %all-gather.18.cloned.1.call-done = bf16[2048,512]{1,0:T(8,128)(2,1)} async-done(((bf16[512,512]{1,0:T(8,128)(2,1)}), bf16[2048,512]{1,0:T(8,128)(2,1)}) %all-gather.18.cloned.1.call-update) | async-done | bytes 2097168 | tf_op jit(solution)/shard_map/all_gather | solution.py:131
  119.0 2.3 fusion.10
  121.3 43.6 %all-gather.20.cloned.1.call-done = bf16[2048,512]{1,0:T(8,128)(2,1)} async-done(((bf16[512,512]{1,0:T(8,128)(2,1)}), bf16[2048,512]{1,0:T(8,128)(2,1)}) %all-gather.20.cloned.1.call-update) | async-done | bytes 2097168 | tf_op jit(solution)/shard_map/all_gather | solution.py:132
  165.0 2.3 fusion.11
  167.3 43.6 %all-gather.22.cloned.1.call-done = bf16[2048,512]{1,0:T(8,128)(2,1)} async-done(((bf16[512,512]{1,0:T(8,128)(2,1)}), bf16[2048,512]{1,0:T(8,128)(2,1)}) %all-gather.22.cloned.1.call-update) | async-done | bytes 2097168 | tf_op jit(solution)/shard_map/all_gather | solution.py:133
  210.9 2.3 fusion.12
  213.2 43.6 %all-gather.24.cloned.1.call-done = bf16[2048,512]{1,0:T(8,128)(2,1)} async-done(((bf16[512,512]{1,0:T(8,128)(2,1)}), bf16[2048,512]{1,0:T(8,128)(2,1)}) %all-gather.24.cloned.1.call-update) | async-done | bytes 2097168 | tf_op jit(solution)/shard_map/all_gather | solution.py:134
  256.8 2.3 fusion.13
  259.4 1.2 fusion.66
  261.5 1.1 reshape.209
  264.2 3.1 fusion.36
  268.1 1.6 fusion.26
  269.6 2.8 fusion.5
  272.6 30.3 %all-gather.26.cloned.1.call-done = bf16[512,2048]{1,0:T(8,128)(2,1)} async-done(((bf16[512,512]{1,0:T(8,128)(2,1)}), bf16[512,2048]{1,0:T(8,128)(2,1)}) %all-gather.26.cloned.1.call-update) | async-done | bytes 2097168 | tf_op jit(solution)/shard_map/all_gather | solution.py:192
  302.9 1.3 collective-permute-start
  306.6 2.9 fusion.35
  309.5 2.0 fusion.4
  313.1 10.9 %all-gather.2 = bf16[4,1,4,4,128]{4,3,2,1,0:T(4,128)(2,1)S(1)} all-gather(bf16[1,1,4,4,128]{4,3,2,1,0:T(4,128)(2,1)S(1)} %slice.110), channel_id=4, replica_groups=mesh['grp'=2,'sp'=4,'tp'=4] {'sp'}, dimensions={0}, use_global_device_ids=true | all-gather | bytes 20480 | tf_op jit(solution)/shard_map/all_gather | solution.py:18
  323.9 10.9 %all-gather = bf16[4,1,4,4,128]{4,3,2,1,0:T(4,128)(2,1)S(1)} all-gather(bf16[1,1,4,4,128]{4,3,2,1,0:T(4,128)(2,1)S(1)} %slice.111), channel_id=2, replica_groups=mesh['grp'=2,'sp'=4,'tp'=4] {'sp'}, dimensions={0}, use_global_device_ids=true | all-gather | bytes 20480 | tf_op jit(solution)/shard_map/all_gather | solution.py:18
  334.8 2.2 convolution_select_fusion
  337.0 1.4 fusion.52
  338.5 1.2 convolution_select_fusion.1
  339.7 5.6 %collective-permute-start.1 = (bf16[512,2048]{1,0:T(8,128)(2,1)S(1)}, bf16[512,2048]{1,0:T(8,128)(2,1)}, u32[]{:S(2)}, u32[]{:S(2)}) collective-permute-start(bf16[512,2048]{1,0:T(8,128)(2,1)S(1)} %collective-permute-done), channel_id=1, source_target_pairs={{0,1},{1,2},{2,3},{3,0},{4,5},{5,6},{6,7},{7,4},{8,9},{9,10},{10,1... | collective-permute-start | bytes 6291464 | tf_op jit(solution)/shard_map/ppermute | solution.py:195
  345.3 1.2 fusion.56
  346.5 2.7 all-gather.30.cloned.1.call-done
  349.4 3.1 fusion.6
  352.5 1.9 rev.19
  354.4 13.9 %collective-permute-done.1 = bf16[512,2048]{1,0:T(8,128)(2,1)} collective-permute-done((bf16[512,2048]{1,0:T(8,128)(2,1)S(1)}, bf16[512,2048]{1,0:T(8,128)(2,1)}, u32[]{:S(2)}, u32[]{:S(2)}) %collective-permute-start.1) | collective-permute-done | bytes 2097184 | tf_op jit(solution)/shard_map/ppermute | solution.py:195
  368.3 2.6 collective-permute-start.2
  370.9 24.6 %all-gather.28.cloned.1.call-done = bf16[16,4,128,128]{3,2,1,0:T(8,128)(2,1)} async-done(((bf16[4,4,128,128]{3,2,1,0:T(8,128)(2,1)}), bf16[16,4,128,128]{3,2,1,0:T(8,128)(2,1)}) %all-gather.28.cloned.1.call-update) | async-done | bytes 2097168 | tf_op jit(solution)/shard_map/all_gather | solution.py:18
  395.6 4.8 %while.26 = (s32[]{:T(128)}, f32[4,4,128,128]{3,2,1,0:T(8,128)S(1)}, s32[]{:T(128)}, bf16[4,4,4,128]{3,2,1,0:T(4,128)(2,1)S(1)}, bf16[4,4,4,128,128]{4,3,2,1,0:T(8,128)(2,1)}, /*index=5*/s32[]{:T(128)}, s32[]{:T(128)}, s32[]{:T(128)}) while((s32[]{:T(128)}, f32[4,4,128,128]{3,2,1,0:T(8,128)S(1)}, s32[]{:T(128)}, ...), condition=%wide.region_3.4_spmd, body=%wide.region_2.3_spmd.sunk | while | flops 788485 | bytes 2642055 | solution.py:33
  395.7 1.5 convert_add_fusion.4
  397.3 1.5 convert_add_fusion.4
  398.9 1.5 convert_add_fusion.4
  400.4 2.6 multiply_reduce_fusion
  404.2 3.9 all-to-all-start
  408.1 5.0 %all-to-all-done = bf16[64,4,512]{2,1,0:T(4,128)(2,1)S(1)} async-done(((bf16[64,4,512]{2,1,0:T(4,128)(2,1)}), bf16[64,4,512]{2,1,0:T(4,128)(2,1)S(1)}, u32[]{:S(2)}, u32[]{:S(2)}) %all-to-all-start) | async-done | bytes 262176 | tf_op jit(solution)/shard_map/all_to_all | solution.py:189
  413.4 1.7 constant_dynamic-update-slice_fusion.7
  415.1 1.7 constant_dynamic-update-slice_fusion.6
  417.0 1.4 copy-done
  418.7 1.7 constant_dynamic-update-slice_fusion.3
  420.4 1.7 constant_dynamic-update-slice_fusion.2
  (89 shorter events, 18.1 us)
Async XLA Ops:
  6.5 7.2 %copy-start.4 = (f32[64,4,512]{2,1,0:T(4,128)S(1)}, f32[64,4,512]{2,1,0:T(4,128)}, u32[]{:S(2)}) copy-start(f32[64,4,512]{2,1,0:T(4,128)} %param.23) | copy-start | bytes 1572868
  6.5 21.3 %all-gather.14.cloned.1.call-start = ((), (), s32[]{:S(2)}) async-start(), calls=%async_computation.1 | async-start | bytes 1310720 | tf_op jit(solution)/shard_map/all_gather | solution.py:136
  9.7 63.3 %all-gather.16.cloned.1.call-start = ((), (), s32[]{:S(2)}) async-start(), calls=%async_computation.2 | async-start | bytes 2621440 | tf_op jit(solution)/shard_map/all_gather | solution.py:130
  10.4 108.6 %all-gather.18.cloned.1.call-start = ((), (), s32[]{:S(2)}) async-start(), calls=%async_computation.3 | async-start | bytes 2621440 | tf_op jit(solution)/shard_map/all_gather | solution.py:131
  11.1 4.0 copy-start.11
  11.2 153.8 %all-gather.20.cloned.1.call-start = ((), (), s32[]{:S(2)}) async-start(), calls=%async_computation.4 | async-start | bytes 2621440 | tf_op jit(solution)/shard_map/all_gather | solution.py:132
  11.7 199.1 %all-gather.22.cloned.1.call-start = ((), (), s32[]{:S(2)}) async-start(), calls=%async_computation.5 | async-start | bytes 2621440 | tf_op jit(solution)/shard_map/all_gather | solution.py:133
  12.3 244.5 %all-gather.24.cloned.1.call-start = ((), (), s32[]{:S(2)}) async-start(), calls=%async_computation.6 | async-start | bytes 2621440 | tf_op jit(solution)/shard_map/all_gather | solution.py:134
  12.9 290.0 %all-gather.26.cloned.1.call-start = ((), (), s32[]{:S(2)}) async-start(), calls=%async_computation.7 | async-start | bytes 2621440 | tf_op jit(solution)/shard_map/all_gather | solution.py:192
  13.6 335.6 %all-gather.30.cloned.1.call-start = ((), (), s32[]{:S(2)}) async-start(), calls=%async_computation.9 | async-start | bytes 2621440 | tf_op jit(solution)/shard_map/all_gather | solution.py:18
  261.0 1.6 copy-start.8
  261.4 2.3 copy-start.9
  262.7 1.4 copy-start.7
  264.1 5.5 %copy-start.2 = (f32[1,64,4,4,128]{4,3,2,1,0:T(4,128)}, f32[1,64,4,4,128]{4,3,2,1,0:T(4,128)S(1)}, u32[]{:S(2)}) copy-start(f32[1,64,4,4,128]{4,3,2,1,0:T(4,128)S(1)} %fusion.28) | copy-start | bytes 1572868
  267.3 0.8 copy-start.1
  272.5 123.0 %all-gather.28.cloned.1.call-start = ((), (), s32[]{:S(2)}) async-start(), calls=%async_computation.8 | async-start | bytes 2621440 | tf_op jit(solution)/shard_map/all_gather | solution.py:18
  302.9 36.8 %collective-permute-start = (bf16[512,2048]{1,0:T(8,128)(2,1)}, bf16[512,2048]{1,0:T(8,128)(2,1)S(1)}, u32[]{:S(2)}, u32[]{:S(2)}) collective-permute-start(bf16[512,2048]{1,0:T(8,128)(2,1)} %all-gather.26.cloned.1.call-done), channel_id=1, source_target_pairs={{0,1},{1,2},{2,3},{3,0},{4,5},{5,6},{6,7},{7,4},{8,9},{9,10},{10,1... | collective-permute-start | bytes 6291464 | tf_op jit(solution)/shard_map/ppermute | solution.py:195
  306.6 28.2 %copy-start.3 = (f32[64,4,4,128]{3,2,1,0:T(4,128)S(1)}, f32[64,4,4,128]{3,2,1,0:T(4,128)}, u32[]{:S(2)}) copy-start(f32[64,4,4,128]{3,2,1,0:T(4,128)} %get-tuple-element.169) | copy-start | bytes 1572868
  311.5 26.9 %copy-start.5 = (f32[64,4,4,128]{3,2,1,0:T(4,128)S(1)}, f32[64,4,4,128]{3,2,1,0:T(4,128)}, u32[]{:S(2)}) copy-start(f32[64,4,4,128]{3,2,1,0:T(4,128)} %get-tuple-element.165) | copy-start | bytes 1572868
  311.5 26.9 %copy-start.6 = (f32[64,4,4,128]{3,2,1,0:T(4,128)S(1)}, f32[64,4,4,128]{3,2,1,0:T(4,128)}, u32[]{:S(2)}) copy-start(f32[64,4,4,128]{3,2,1,0:T(4,128)} %get-tuple-element.172) | copy-start | bytes 1572868
  339.7 28.6 %collective-permute-start.1 = (bf16[512,2048]{1,0:T(8,128)(2,1)S(1)}, bf16[512,2048]{1,0:T(8,128)(2,1)}, u32[]{:S(2)}, u32[]{:S(2)}) collective-permute-start(bf16[512,2048]{1,0:T(8,128)(2,1)S(1)} %collective-permute-done), channel_id=1, source_target_pairs={{0,1},{1,2},{2,3},{3,0},{4,5},{5,6},{6,7},{7,4},{8,9},{9,10},{10,1... | collective-permute-start | bytes 6291464 | tf_op jit(solution)/shard_map/ppermute | solution.py:195
  368.3 45.1 %collective-permute-start.2 = (bf16[512,2048]{1,0:T(8,128)(2,1)}, bf16[512,2048]{1,0:T(8,128)(2,1)}, u32[]{:S(2)}, u32[]{:S(2)}) collective-permute-start(bf16[512,2048]{1,0:T(8,128)(2,1)} %collective-permute-done.1), channel_id=1, source_target_pairs={{0,1},{1,2},{2,3},{3,0},{4,5},{5,6},{6,7},{7,4},{8,9},{9,10},{10,1... | collective-permute-start | bytes 6291464 | tf_op jit(solution)/shard_map/ppermute | solution.py:195
  400.4 2.6 copy-start.10
  400.4 2.6 copy-start.12
  404.2 8.9 %all-to-all-start = ((bf16[64,4,512]{2,1,0:T(4,128)(2,1)}), bf16[64,4,512]{2,1,0:T(4,128)(2,1)S(1)}, u32[]{:S(2)}, u32[]{:S(2)}) async-start(bf16[64,4,512]{2,1,0:T(4,128)(2,1)} %copy.53), calls=%async_computation | async-start | bytes 524288 | tf_op jit(solution)/shard_map/all_to_all | solution.py:189
  416.9 1.6 copy-start
Sparse Core Ops, SparseCore 0:
  9.8 18.0 all-gather.13
  29.4 43.4 all-gather.15
  74.5 44.4 all-gather.17
  120.5 44.4 all-gather.19
  166.4 44.4 all-gather.21
  212.3 44.4 all-gather.23
  258.4 44.4 all-gather.25
  304.4 44.7 all-gather.29
  350.8 44.6 all-gather.27
